TPU v7x, 32 devices: a whole 2x2x4 slice. The times are simulated.
32 devices in a mesh: sp: 4 (over z), dp: 8 (over y, x, core).
Axes of the slice: x: 2, y: 2, z: 4, core: 2. Of those that a mesh axis runs over, the one named last changes fastest.
Arguments:
- tokens: bfloat16 [16, 256, 1024], P('dp', 'sp'), may hold values from -6 to 6
- norm_gain: float32 [1024], replicated, may hold values from 0.1 to 1.9
- w_query: bfloat16 [1024, 128], P('dp'), may hold values from -0.1875 to 0.1875
- w_key: bfloat16 [1024, 128], P('dp'), may hold values from -0.1875 to 0.1875
- w_value: bfloat16 [1024, 128], P('dp'), may hold values from -0.1875 to 0.1875
- w_rank_forward: bfloat16 [1024, 16], P('dp'), may hold values from -0.1875 to 0.1875
- w_rank_backward: bfloat16 [1024, 16], P('dp'), may hold values from -0.1875 to 0.1875
- up_forward: bfloat16 [16, 128], replicated, may hold values from -1.5 to 1.5
- up_backward: bfloat16 [16, 128], replicated, may hold values from -1.5 to 1.5
- bias_forward: float32 [128], replicated, may hold values from -1.5 to 3
- bias_backward: float32 [128], replicated, may hold values from -1.5 to 3
- out_gain: float32 [32], replicated, may hold values from 0.1 to 1.9
- w_out: bfloat16 [128, 1024], P('dp'), may hold values from -0.5 to 0.5
Outputs:
- mixed_out: bfloat16 [16, 256, 1024], P('dp', 'sp')
All inputs are finite; a program needn't handle non-finite values.
Results may differ from a plain program's by a relative error of at most 0.005.
Values may be sent and summed in bfloat16 or wider, within the bound.
A program may use at most 64 MiB of HBM per device.

v0:
```python
import jax
import jax.numpy as jnp
from jax import lax
from jax.sharding import PartitionSpec as P

HK = 32
HV = 32
BLOCK = 64


eps = 1e-06
precise = lax.Precision.HIGHEST


def over_all(x, axis, dim, take_in, carry):
    whole = jax.tree.map(lambda part: lax.all_gather(part, axis, axis=dim, tiled=True), x)
    return take_in(carry, whole, jnp.int32(0))


def for_sending(x):
    return jax.tree.map(lambda a: a.astype(jnp.bfloat16) if a.dtype == jnp.float32 else a, x)


def rms_norm(values, norm_scale):
    return values * lax.rsqrt(jnp.mean(values * values, axis=-1, keepdims=True) + eps) * norm_scale


def one_way(queries, key_rows, value_rows, decay_rates):
    head_count, length, key_width = queries.shape
    value_width = value_rows.shape[-1]
    blocks = length // BLOCK

    def in_blocks(tensor):
        return tensor.reshape(head_count, blocks, BLOCK, tensor.shape[-1])

    query_blocks = in_blocks(queries)
    key_blocks = in_blocks(key_rows)
    value_blocks = in_blocks(value_rows)
    running = jnp.cumsum(in_blocks(decay_rates), axis=2)
    closing = running[:, :, -1:, :]
    query_decayed = query_blocks * jnp.exp(running)
    key_inverse = key_blocks * jnp.exp(-running)
    key_remain = key_blocks * jnp.exp(closing - running)
    triangle = jnp.tril(jnp.ones((BLOCK, BLOCK), jnp.float32))
    scores = jnp.einsum("hnid,hnjd->hnij", query_decayed, key_inverse, precision=precise) * triangle
    within = jnp.einsum("hnij,hnjv->hniv", scores, value_blocks, precision=precise)
    block_decay = jnp.exp(closing[:, :, 0, :])

    def advance(carried, inputs):
        query_now, key_now, value_now, decay_now = inputs
        emitted = jnp.einsum("hid,hdv->hiv", query_now, carried, precision=precise)
        carried = decay_now[..., None] * carried + jnp.einsum(
            "hid,hiv->hdv", key_now, value_now, precision=precise
        )
        return (carried, emitted)

    initial = jnp.zeros((head_count, key_width, value_width), jnp.float32)
    stacked = tuple(
        (
            jnp.moveaxis(tensor, 1, 0)
            for tensor in (query_decayed, key_remain, value_blocks, block_decay)
        )
    )
    final_state, across = lax.scan(advance, initial, stacked)
    return (within + jnp.moveaxis(across, 0, 1)).reshape(head_count, length, value_width)


def both_ways(queries, key_rows, value_rows, rates_forward, rates_backward):
    forward = one_way(queries, key_rows, value_rows, rates_forward)
    backward = one_way(
        jnp.flip(queries, 1),
        jnp.flip(key_rows, 1),
        jnp.flip(value_rows, 1),
        jnp.flip(rates_backward, 1),
    )
    return forward + jnp.flip(backward, 1)


def by_head(tensor, head_width):
    length = tensor.shape[0]
    return tensor.reshape(length, -1, head_width).transpose(1, 0, 2).astype(jnp.float32)


def attend(queries, key_rows, value_rows, rates_forward, rates_backward, out_gain):
    combined = both_ways(
        by_head(queries, HK) * HK ** (-0.5),
        by_head(key_rows, HK),
        by_head(value_rows, HV),
        by_head(rates_forward, HK),
        by_head(rates_backward, HK),
    )
    normed = rms_norm(combined, out_gain).astype(jnp.bfloat16)
    return normed.transpose(1, 0, 2).reshape(normed.shape[1], -1)


def per_device(
    tokens,
    norm_gain,
    w_query,
    w_key,
    w_value,
    w_rank_forward,
    w_rank_backward,
    up_forward,
    up_backward,
    bias_forward,
    bias_backward,
    out_gain,
    w_out,
):
    seq_local, tok_local, model_width = tokens.shape
    sp_count = lax.axis_size("sp")
    length = tok_local * sp_count
    rate_scale = 2.0 / length
    row_count = seq_local * tok_local
    normed = rms_norm(tokens.reshape(row_count, model_width).astype(jnp.float32), norm_gain).astype(
        jnp.bfloat16
    )

    def add_rows(totals, pieces, offset):
        span_rows = pieces[0].shape[0]
        left_part = lax.dynamic_slice_in_dim(normed, offset, span_rows, 1)
        return tuple(
            (
                running_sum + jnp.dot(left_part, shard_piece, preferred_element_type=jnp.float32)
                for running_sum, shard_piece in zip(totals, pieces)
            )
        )

    starting = tuple(
        (
            jnp.zeros((row_count, weight.shape[1]), jnp.float32)
            for weight in (w_query, w_key, w_value, w_rank_forward, w_rank_backward)
        )
    )
    projected = over_all(
        (w_query, w_key, w_value, w_rank_forward, w_rank_backward), "dp", 0, add_rows, starting
    )
    queries = projected[0].astype(jnp.bfloat16).reshape(seq_local, tok_local, -1)
    key_rows = projected[1].astype(jnp.bfloat16).reshape(seq_local, tok_local, -1)
    value_rows = projected[2].astype(jnp.bfloat16).reshape(seq_local, tok_local, -1)
    rank_forward = projected[3].astype(jnp.bfloat16)
    rank_backward = projected[4].astype(jnp.bfloat16)
    head_queries, head_keys, head_values = (
        lax.all_to_all(queries, "sp", split_axis=2, concat_axis=1, tiled=True),
        lax.all_to_all(key_rows, "sp", split_axis=2, concat_axis=1, tiled=True),
        lax.all_to_all(value_rows, "sp", split_axis=2, concat_axis=1, tiled=True),
    )
    own_forward = (
        jax.nn.log_sigmoid(
            jnp.dot(rank_forward, up_forward, preferred_element_type=jnp.float32) + bias_forward
        )
        * rate_scale
    )
    own_backward = (
        jax.nn.log_sigmoid(
            jnp.dot(rank_backward, up_backward, preferred_element_type=jnp.float32) + bias_backward
        )
        * rate_scale
    )
    rates_forward, rates_backward = (
        lax.all_to_all(
            for_sending(own_forward.reshape(seq_local, tok_local, -1)),
            "sp",
            split_axis=2,
            concat_axis=1,
            tiled=True,
        ),
        lax.all_to_all(
            for_sending(own_backward.reshape(seq_local, tok_local, -1)),
            "sp",
            split_axis=2,
            concat_axis=1,
            tiled=True,
        ),
    )
    attended = jax.vmap(attend, in_axes=(0, 0, 0, 0, 0, None))(
        head_queries, head_keys, head_values, rates_forward, rates_backward, out_gain
    )
    gathered_heads = jax.tree.map(
        lambda part, own: part.astype(own.dtype),
        lax.all_to_all(for_sending(attended), "sp", split_axis=1, concat_axis=2, tiled=True),
        attended,
    ).reshape(row_count, -1)

    def add_out(running_sum, shard_piece, offset):
        left_part = lax.dynamic_slice_in_dim(gathered_heads, offset, shard_piece.shape[0], 1)
        return running_sum + jnp.dot(left_part, shard_piece, preferred_element_type=jnp.float32)

    mixed_out = over_all(
        w_out, "dp", 0, add_out, jnp.zeros((row_count, w_out.shape[1]), jnp.float32)
    )
    return mixed_out.astype(jnp.bfloat16).reshape(seq_local, tok_local, -1)


def solution(mesh):
    return jax.shard_map(
        per_device,
        mesh=mesh,
        in_specs=(
            P("dp", "sp", None),
            P(),
            P("dp", None),
            P("dp", None),
            P("dp", None),
            P("dp", None),
            P("dp", None),
            P(),
            P(),
            P(),
            P(),
            P(),
            P("dp", None),
        ),
        out_specs=P("dp", "sp", None),
        check_vma=False,
    )
```

profile of v0, /device:TPU:0, one launch (start us, length us, event | category | flops | bytes accessed | tf_op | source)
XLA Modules:
  0.0 118.0 jit_solution(11206527147901036018)
XLA Ops:
  0.0 1.2 multiply_reduce_fusion
  1.3 11.2 %all_gather.18 = bf16[1024,128]{1,0:T(8,128)(2,1)S(1)} all-gather(bf16[128,128]{1,0:T(8,128)(2,1)} %param.19), channel_id=1, replica_groups=mesh['sp'=4,'dp'=8] {'dp'}, dimensions={0}, use_global_device_ids=true | all-gather | bytes 294912 | tf_op jit(solution)/shard_map/all_gather | solution.py:16
  12.6 0.2 convolution_convert_fusion.3
  12.9 0.7 reshape.393
  13.6 5.0 %all-to-all-start = ((bf16[4,2,2048]{2,1,0:T(2,128)(2,1)}), bf16[4,2,2048]{2,1,0:T(2,128)(2,1)S(1)}, u32[]{:S(2)}, u32[]{:S(2)}) async-start(bf16[4,2,2048]{2,1,0:T(2,128)(2,1)} %reshape.393), calls=%async_computation | async-start | bytes 65536 | tf_op jit(solution)/shard_map/all_to_all | solution.py:145
  18.6 9.1 %all_gather.20 = bf16[1024,128]{1,0:T(8,128)(2,1)S(1)} all-gather(bf16[128,128]{1,0:T(8,128)(2,1)S(1)} %copy-done.2), channel_id=1, replica_groups=mesh['sp'=4,'dp'=8] {'dp'}, dimensions={0}, use_global_device_ids=true | all-gather | bytes 294912 | tf_op jit(solution)/shard_map/all_gather | solution.py:16
  27.7 0.2 convolution_convert_fusion.2
  27.9 0.5 copy-done.6
  28.4 8.2 %all_gather.19 = bf16[1024,16]{0,1:T(8,128)(2,1)S(1)} all-gather(bf16[128,16]{0,1:T(8,128)(2,1)S(1)} %copy-done.6), channel_id=1, replica_groups=mesh['sp'=4,'dp'=8] {'dp'}, dimensions={0}, use_global_device_ids=true | all-gather | bytes 36864 | tf_op jit(solution)/shard_map/all_gather | solution.py:16
  36.6 9.1 %all_gather.21 = bf16[1024,128]{1,0:T(8,128)(2,1)S(1)} all-gather(bf16[128,128]{1,0:T(8,128)(2,1)S(1)} %copy-done.3), channel_id=1, replica_groups=mesh['sp'=4,'dp'=8] {'dp'}, dimensions={0}, use_global_device_ids=true | all-gather | bytes 294912 | tf_op jit(solution)/shard_map/all_gather | solution.py:16
  45.6 0.2 convolution_convert_fusion.1
  45.9 0.5 copy-done.7
  46.3 8.2 %all_gather.22 = bf16[1024,16]{0,1:T(8,128)(2,1)S(1)} all-gather(bf16[128,16]{0,1:T(8,128)(2,1)S(1)} %copy-done.7), channel_id=1, replica_groups=mesh['sp'=4,'dp'=8] {'dp'}, dimensions={0}, use_global_device_ids=true | all-gather | bytes 36864 | tf_op jit(solution)/shard_map/all_gather | solution.py:16
  54.5 0.4 fusion.47
  54.9 0.3 copy-done.9
  55.2 0.4 fusion.50
  55.8 0.7 reshape.389
  56.6 0.7 reshape.391
  57.5 0.7 reshape.387
  58.3 0.7 reshape.395
  59.1 5.1 %all-to-all-start.1 = ((bf16[4,2,2048]{2,1,0:T(2,128)(2,1)}), bf16[4,2,2048]{2,1,0:T(2,128)(2,1)S(1)}, u32[]{:S(2)}, u32[]{:S(2)}) async-start(bf16[4,2,2048]{2,1,0:T(2,128)(2,1)} %reshape.391), calls=%async_computation.1 | async-start | bytes 65536 | tf_op jit(solution)/shard_map/all_to_all | solution.py:162
  64.3 5.5 %all-to-all-done.1 = bf16[4,2,2048]{2,1,0:T(2,128)(2,1)S(1)} async-done(((bf16[4,2,2048]{2,1,0:T(2,128)(2,1)}), bf16[4,2,2048]{2,1,0:T(2,128)(2,1)S(1)}, u32[]{:S(2)}, u32[]{:S(2)}) %all-to-all-start.1) | async-done | bytes 32800 | tf_op jit(solution)/shard_map/all_to_all | solution.py:162
  69.8 3.3 %all-to-all-start.2 = ((bf16[4,2,2048]{2,1,0:T(2,128)(2,1)}), bf16[4,2,2048]{2,1,0:T(2,128)(2,1)S(1)}, u32[]{:S(2)}, u32[]{:S(2)}) async-start(bf16[4,2,2048]{2,1,0:T(2,128)(2,1)} %reshape.389), calls=%async_computation.2 | async-start | bytes 65536 | tf_op jit(solution)/shard_map/all_to_all | solution.py:146
  73.3 5.5 %all-to-all-done.2 = bf16[4,2,2048]{2,1,0:T(2,128)(2,1)S(1)} async-done(((bf16[4,2,2048]{2,1,0:T(2,128)(2,1)}), bf16[4,2,2048]{2,1,0:T(2,128)(2,1)S(1)}, u32[]{:S(2)}, u32[]{:S(2)}) %all-to-all-start.2) | async-done | bytes 32800 | tf_op jit(solution)/shard_map/all_to_all | solution.py:146
  78.7 3.3 %all-to-all-start.3 = ((bf16[4,2,2048]{2,1,0:T(2,128)(2,1)}), bf16[4,2,2048]{2,1,0:T(2,128)(2,1)S(1)}, u32[]{:S(2)}, u32[]{:S(2)}) async-start(bf16[4,2,2048]{2,1,0:T(2,128)(2,1)} %reshape.387), calls=%async_computation.3 | async-start | bytes 65536 | tf_op jit(solution)/shard_map/all_to_all | solution.py:147
  82.5 5.1 %all-to-all-done.3 = bf16[4,2,2048]{2,1,0:T(2,128)(2,1)S(1)} async-done(((bf16[4,2,2048]{2,1,0:T(2,128)(2,1)}), bf16[4,2,2048]{2,1,0:T(2,128)(2,1)S(1)}, u32[]{:S(2)}, u32[]{:S(2)}) %all-to-all-start.3) | async-done | bytes 32800 | tf_op jit(solution)/shard_map/all_to_all | solution.py:147
  87.6 3.3 %all-to-all-start.4 = ((bf16[4,2,2048]{2,1,0:T(2,128)(2,1)}), bf16[4,2,2048]{2,1,0:T(2,128)(2,1)S(1)}, u32[]{:S(2)}, u32[]{:S(2)}) async-start(bf16[4,2,2048]{2,1,0:T(2,128)(2,1)} %reshape.395), calls=%async_computation.4 | async-start | bytes 65536 | tf_op jit(solution)/shard_map/all_to_all | solution.py:169
  91.0 0.3 reduce_window_sum.19
  91.3 0.6 convolution_multiply_fusion.1
  92.3 1.8 %while.26 = (s32[]{:T(128)}, f32[2,1,32,32]{3,2,0,1:T(8,128)S(1)}, f32[4,2,1,64,32]{3,4,0,1,2:T(8,128)S(1)}, f32[4,2,1,32]{3,0,1,2:T(4,128)S(1)}, f32[4,2,1,64,3...) while((s32[]{:T(128)}, f32[2,1,32,32]{3,2,0,1:T(8,128)S(1)}, ...), condition=%wide.region_3.4_spmd.clone, body=%wide.region_2.3_spmd.clone.sunk | while | flops 3153923 | bytes 209522 | solution.py:64
  92.3 0.2 fusion.90
  92.5 0.2 fusion.89
  92.7 0.2 fusion.90
  93.0 0.2 fusion.89
  93.2 0.2 fusion.90
  93.4 0.2 fusion.89
  93.6 0.2 fusion.90
  93.9 0.2 fusion.89
  94.2 0.1 reshape.369
  94.3 0.2 reverse.3
  94.5 0.3 fusion.28
  94.9 0.1 reshape.372
  95.0 0.2 rev.19
  95.5 0.1 reshape.356
  95.9 0.6 all-to-all-done.4
  96.9 0.2 rev.17
  97.2 0.3 reduce_window_sum.21
  97.8 2.0 %while.27 = (s32[]{:T(128)}, f32[2,1,32,32]{3,2,0,1:T(8,128)S(1)}, f32[4,2,1,64,32]{3,4,0,1,2:T(8,128)S(1)}, f32[4,2,1,32]{3,0,1,2:T(4,128)S(1)}, f32[4,2,1,64,3...) while((s32[]{:T(128)}, f32[2,1,32,32]{3,2,0,1:T(8,128)S(1)}, ...), condition=%wide.region_6.7_spmd.clone, body=%wide.region_5.6_spmd.clone.sunk | while | flops 3153923 | bytes 240763 | solution.py:64
  97.8 0.2 fusion.96
  98.1 0.2 fusion.95
  98.3 0.2 fusion.96
  98.6 0.2 fusion.95
  98.8 0.2 fusion.96
  99.1 0.2 fusion.95
  99.3 0.2 fusion.96
  99.6 0.2 fusion.95
  99.8 0.6 convolution_multiply_fusion
  100.4 0.5 fusion.29
  101.2 0.2 rev.20
  101.4 0.6 copy-done.8
  102.2 0.8 reshape.397
  103.0 4.6 %all-to-all-start.5 = ((bf16[4,2,2048]{2,1,0:T(2,128)(2,1)}), bf16[4,2,2048]{2,1,0:T(2,128)(2,1)S(1)}, u32[]{:S(2)}, u32[]{:S(2)}) async-start(bf16[4,2,2048]{2,1,0:T(2,128)(2,1)} %reshape.397), calls=%async_computation.5 | async-start | bytes 65536 | tf_op jit(solution)/shard_map/all_to_all | solution.py:182
  107.6 9.1 %all_gather.23 = bf16[128,1024]{1,0:T(8,128)(2,1)S(1)} all-gather(bf16[16,1024]{1,0:T(8,128)(2,1)S(1)} %copy-done.4), channel_id=1, replica_groups=mesh['sp'=4,'dp'=8] {'dp'}, dimensions={0}, use_global_device_ids=true | all-gather | bytes 294912 | tf_op jit(solution)/shard_map/all_gather | solution.py:16
  117.0 1.0 convolution_convert_fusion
  (92 shorter events, 4.7 us)
Async XLA Ops:
  0.0 54.5 %copy-start = (bf16[16,128]{1,0:T(8,128)(2,1)S(1)}, bf16[16,128]{1,0:T(8,128)(2,1)}, u32[]{:S(2)}) copy-start(bf16[16,128]{1,0:T(8,128)(2,1)} %param.24) | copy-start | bytes 12292
  0.0 12.4 %copy-start.1 = (bf16[2,64,1024]{2,1,0:T(8,128)(2,1)S(1)}, bf16[2,64,1024]{2,1,0:T(8,128)(2,1)}, u32[]{:S(2)}) copy-start(bf16[2,64,1024]{2,1,0:T(8,128)(2,1)} %param.17) | copy-start | bytes 786436
  1.3 11.2 %copy-start.5 = (f32[1024]{0:T(1024)S(1)}, f32[1024]{0:T(1024)}, u32[]{:S(2)}) copy-start(f32[1024]{0:T(1024)} %param.18) | copy-start | bytes 12292
  13.6 5.0 %copy-start.2 = (bf16[128,128]{1,0:T(8,128)(2,1)S(1)}, bf16[128,128]{1,0:T(8,128)(2,1)}, u32[]{:S(2)}) copy-start(bf16[128,128]{1,0:T(8,128)(2,1)} %param.20) | copy-start | bytes 98308
  13.6 45.4 %all-to-all-start = ((bf16[4,2,2048]{2,1,0:T(2,128)(2,1)}), bf16[4,2,2048]{2,1,0:T(2,128)(2,1)S(1)}, u32[]{:S(2)}, u32[]{:S(2)}) async-start(bf16[4,2,2048]{2,1,0:T(2,128)(2,1)} %reshape.393), calls=%async_computation | async-start | bytes 65536 | tf_op jit(solution)/shard_map/all_to_all | solution.py:145
  27.7 0.7 copy-start.6
  28.4 8.2 %copy-start.3 = (bf16[128,128]{1,0:T(8,128)(2,1)S(1)}, bf16[128,128]{1,0:T(8,128)(2,1)}, u32[]{:S(2)}) copy-start(bf16[128,128]{1,0:T(8,128)(2,1)} %param.21) | copy-start | bytes 98308
  45.6 0.7 copy-start.7
  46.3 8.2 %copy-start.10 = (f32[128]{0:T(128)S(1)}, f32[128]{0:T(128)}, u32[]{:S(2)}) copy-start(f32[128]{0:T(128)} %param.26) | copy-start | bytes 1540
  54.5 0.7 copy-start.9
  54.5 0.7 copy-start.11
  59.1 10.7 %all-to-all-start.1 = ((bf16[4,2,2048]{2,1,0:T(2,128)(2,1)}), bf16[4,2,2048]{2,1,0:T(2,128)(2,1)S(1)}, u32[]{:S(2)}, u32[]{:S(2)}) async-start(bf16[4,2,2048]{2,1,0:T(2,128)(2,1)} %reshape.391), calls=%async_computation.1 | async-start | bytes 65536 | tf_op jit(solution)/shard_map/all_to_all | solution.py:162
  69.8 8.9 %all-to-all-start.2 = ((bf16[4,2,2048]{2,1,0:T(2,128)(2,1)}), bf16[4,2,2048]{2,1,0:T(2,128)(2,1)S(1)}, u32[]{:S(2)}, u32[]{:S(2)}) async-start(bf16[4,2,2048]{2,1,0:T(2,128)(2,1)} %reshape.389), calls=%async_computation.2 | async-start | bytes 65536 | tf_op jit(solution)/shard_map/all_to_all | solution.py:146
  78.7 8.9 %all-to-all-start.3 = ((bf16[4,2,2048]{2,1,0:T(2,128)(2,1)}), bf16[4,2,2048]{2,1,0:T(2,128)(2,1)S(1)}, u32[]{:S(2)}, u32[]{:S(2)}) async-start(bf16[4,2,2048]{2,1,0:T(2,128)(2,1)} %reshape.387), calls=%async_computation.3 | async-start | bytes 65536 | tf_op jit(solution)/shard_map/all_to_all | solution.py:147
  87.6 8.9 %all-to-all-start.4 = ((bf16[4,2,2048]{2,1,0:T(2,128)(2,1)}), bf16[4,2,2048]{2,1,0:T(2,128)(2,1)S(1)}, u32[]{:S(2)}, u32[]{:S(2)}) async-start(bf16[4,2,2048]{2,1,0:T(2,128)(2,1)} %reshape.395), calls=%async_computation.4 | async-start | bytes 65536 | tf_op jit(solution)/shard_map/all_to_all | solution.py:169
  101.4 0.7 copy-start.8
  103.0 4.6 %copy-start.4 = (bf16[16,1024]{1,0:T(8,128)(2,1)S(1)}, bf16[16,1024]{1,0:T(8,128)(2,1)}, u32[]{:S(2)}) copy-start(bf16[16,1024]{1,0:T(8,128)(2,1)} %param.29) | copy-start | bytes 98308
  103.0 13.7 %all-to-all-start.5 = ((bf16[4,2,2048]{2,1,0:T(2,128)(2,1)}), bf16[4,2,2048]{2,1,0:T(2,128)(2,1)S(1)}, u32[]{:S(2)}, u32[]{:S(2)}) async-start(bf16[4,2,2048]{2,1,0:T(2,128)(2,1)} %reshape.397), calls=%async_computation.5 | async-start | bytes 65536 | tf_op jit(solution)/shard_map/all_to_all | solution.py:182
where the time goes:
time: 119 us; the launch traced here: 118 us
  blocking collectives  54.7 us (46%)
  starting transfers between devices  24.5 us (21%)
  waiting for transfers between devices  16.7 us (14%)
  local copies, waits for them, and re-layouts  11.5 us (10%)
  matrix products  7.7 us (6%)
  other arithmetic  2.15 us (2%)
    all_gather x6, blocking collectives, over_all(): lax.all_gather(part, axis, axis=dim, tiled=True)  54.7 us
    unnamed x40, local copies, waits for them, and re-layouts  7.47 us
    all_to_all x1, waiting for transfers between devices, per_device(): lax.all_to_all(for_sending(own_forward.reshape(seq_local, tok_local, -1))...  5.52 us
    all_to_all x1, waiting for transfers between devices, per_device(): lax.all_to_all(key_rows, 'sp', split_axis=2, concat_axis=1, tiled=True)  5.47 us
    all_to_all x1, starting transfers between devices, per_device(): lax.all_to_all(for_sending(own_forward.reshape(seq_local, tok_local, -1))...  5.09 us
    all_to_all x1, waiting for transfers between devices, per_device(): lax.all_to_all(value_rows, 'sp', split_axis=2, concat_axis=1, tiled=True)  5.08 us
    all_to_all x1, starting transfers between devices, per_device(): lax.all_to_all(queries, 'sp', split_axis=2, concat_axis=1, tiled=True)  5 us
    all_to_all x1, starting transfers between devices, per_device(): lax.all_to_all(for_sending(attended), 'sp', split_axis=1, concat_axis=2,...  4.6 us
  transfers between devices with their start and end apart: 6, of which 4 were waited for; matrix products, arithmetic and copies ran while one was open for 9% of the time, Pallas kernels for 0%

commit v1 on v0

v1 whole, which is shorter than its diff:
```python
import functools

import jax
import jax.numpy as jnp
from jax import lax
from jax.experimental import pallas as pl
from jax.experimental.pallas import tpu as pltpu
from jax.sharding import PartitionSpec as P

HK = 32
LANES = 128
EPS = 1e-06
f32 = jnp.float32
bf16 = jnp.bfloat16


def dot(a, b, dims=((1,), (0,))):
    return lax.dot_general(a, b, (dims, ((), ())), preferred_element_type=f32)


def split_dot(a, b):
    high = b.astype(bf16)
    low = (b - high.astype(f32)).astype(bf16)
    return dot(a, high) + dot(a, low)


def kernel(
    n_sp,
    n_dp,
    tokens,
    norm_gain,
    w_query,
    w_key,
    w_value,
    w_rank_f,
    w_rank_b,
    up_f,
    up_b,
    bias_f,
    bias_b,
    out_gain,
    w_out,
    result,
    tok_v,
    gain_v,
    rank_v,
    up_v,
    bias_v,
    ogain_v,
    wr,
    wk,
    wv,
    wq,
    wo,
    states,
    inbox,
    local_sem,
    send_sem,
    relay_sem,
    recv_sem,
    sp_send_sem,
    sp_recv_sem,
):
    sp = lax.axis_index("sp")
    dp = lax.axis_index("dp")
    chips = n_dp // 2
    core = lax.rem(dp, 2)
    chip = lax.div(dp, 2)
    partner = chip * 2 + (1 - core)
    seqs, toks, width = tok_v.shape
    rows = seqs * toks
    depth = w_query.shape[0]
    out_depth = w_out.shape[0]
    keys = w_query.shape[1]
    rank = w_rank_f.shape[1]
    groups = keys // LANES
    heads = LANES // HK

    def slot(which, src):
        ref = (wr, wk, wv, wq, wo)[which]
        if which == 0:
            return ref.at[src]
        size = out_depth if which == 4 else depth
        return ref.at[pl.ds(pl.multiple_of(src * size, size), size), :]

    barrier = pltpu.get_barrier_semaphore()
    far = [lax.rem(chip + s, chips) * 2 + core for s in range(1, chips)]
    peers = [lax.rem(sp + s, n_sp) for s in range(1, n_sp)]
    for d in far + [partner]:
        pl.semaphore_signal(barrier, inc=1, device_id={"dp": d})
    for p in peers:
        pl.semaphore_signal(barrier, inc=1, device_id={"sp": p})

    loads = []
    for src, dst in (
        (w_rank_f, rank_v.at[0]),
        (w_rank_b, rank_v.at[1]),
        (w_key, slot(1, dp)),
        (w_value, slot(2, dp)),
        (w_query, slot(3, dp)),
        (tokens, tok_v),
        (norm_gain, gain_v),
        (w_out, slot(4, dp)),
        (up_f, up_v.at[0]),
        (up_b, up_v.at[1]),
        (bias_f, bias_v.at[0]),
        (bias_b, bias_v.at[1]),
        (out_gain, ogain_v),
    ):
        copy = pltpu.make_async_copy(src, dst, local_sem.at[len(loads)])
        copy.start()
        loads.append(copy)
    inbox[sp] = jnp.zeros(inbox.shape[1:], bf16)
    loads[0].wait()
    loads[1].wait()
    wr[dp] = jnp.concatenate([rank_v[0].astype(f32).T, rank_v[1].astype(f32).T], axis=0).astype(bf16)
    pl.semaphore_wait(barrier, len(far) + 1 + len(peers))

    def remote(which, src, sem, target):
        return pltpu.make_async_remote_copy(
            src_ref=slot(which, src),
            dst_ref=slot(which, src),
            send_sem=sem,
            recv_sem=recv_sem.at[which, src],
            device_id={"dp": target},
        )

    sends = []
    waits = {1: 2, 2: 3, 3: 4, 4: 7}
    for which in range(5):
        if which:
            loads[waits[which]].wait()
        for i, d in enumerate(far):
            copy = remote(which, dp, send_sem.at[which, i], d)
            copy.start()
            sends.append(copy)
        copy = remote(which, dp, relay_sem.at[which, 0], partner)
        copy.start()
        sends.append(copy)

    loads[5].wait()
    loads[6].wait()
    x = tok_v[...].reshape(rows, width).astype(f32)
    normed = (x * lax.rsqrt(jnp.mean(x * x, axis=-1, keepdims=True) + EPS) * gain_v[...]).astype(bf16)

    for copy in loads[8:]:
        copy.wait()

    def relay(which):
        for i in range(1, chips):
            src = lax.rem(chip + chips - i, chips) * 2 + core
            remote(which, src, relay_sem.at[which, i], partner).wait_recv()
            copy = remote(which, src, relay_sem.at[which, i], partner)
            copy.start()
            sends.append(copy)

    def arrive(which):
        for i in range(chips):
            src = lax.rem(chip + chips - i, chips) * 2 + (1 - core)
            remote(which, src, relay_sem.at[which, i], partner).wait_recv()

    row = lax.broadcasted_iota(jnp.int32, (rows, rows), 0)
    col = lax.broadcasted_iota(jnp.int32, (rows, rows), 1)
    same = lax.div(row, toks) == lax.div(col, toks)
    lower = jnp.where(same & (row >= col), 1.0, 0.0).astype(bf16)
    upper = jnp.where(same & (row <= col), 1.0, 0.0).astype(bf16)

    relay(0)
    arrive(0)
    w_ranks = jnp.concatenate([wr[s] for s in range(n_dp)], axis=1)
    ranks = dot(normed, w_ranks, ((1,), (1,))).astype(bf16)
    scale = 2.0 / (toks * n_sp)
    running = []
    for d in range(2):
        logits = dot(ranks[:, d * rank : (d + 1) * rank], up_v[d]) + bias_v[d]
        rates = (jnp.minimum(logits, 0.0) - jnp.log1p(jnp.exp(-jnp.abs(logits)))) * scale
        running.append(split_dot(upper if d else lower, rates))
    relay(1)
    arrive(1)
    k = dot(normed, wk[...]).astype(bf16).astype(f32)
    relay(2)
    arrive(2)
    v = dot(normed, wv[...]).astype(bf16)

    lane = lax.broadcasted_iota(jnp.int32, (1, LANES), 1)
    head_mask = [jnp.where(lax.div(lane, HK) == h, 1.0, 0.0) for h in range(heads)]
    head_mask16 = [m.astype(bf16) for m in head_mask]
    tag_row = lax.broadcasted_iota(jnp.int32, (16, LANES), 0)

    def part(a, b, g):
        return a[b * toks : (b + 1) * toks, g * LANES : (g + 1) * LANES]

    closing = {}
    for b in range(seqs):
        for g in range(groups):
            for d in range(2):
                run = part(running[d], b, g)
                end = run[:1] if d else run[toks - 1 :]
                remain = (part(k, b, g) * jnp.exp(end - run)).astype(bf16)
                summary = dot(remain, part(v, b, g), ((0,), (0,)))
                packed = sum(summary[h * HK : (h + 1) * HK] * head_mask[h] for h in range(heads))
                high = end.astype(bf16).astype(f32)
                tags = jnp.where(tag_row == 0, high, jnp.where(tag_row == 1, end - high, 0.0))
                states[d, b * groups + g] = jnp.concatenate([packed, tags], axis=0).astype(bf16)
    for i, p in enumerate(peers):
        back = jnp.where(p < sp, 1, 0)
        copy = pltpu.make_async_remote_copy(
            src_ref=states.at[back],
            dst_ref=inbox.at[sp],
            send_sem=sp_send_sem.at[i],
            recv_sem=sp_recv_sem.at[sp],
            device_id={"sp": p},
        )
        copy.start()
        sends.append(copy)

    relay(3)
    arrive(3)
    q = dot(normed, wq[...]).astype(bf16).astype(f32) * HK ** (-0.5)
    relay(4)

    t_row = lax.broadcasted_iota(jnp.int32, (toks, heads * toks), 0)
    t_col = lax.rem(lax.broadcasted_iota(jnp.int32, (toks, heads * toks), 1), toks)
    decayed = {}
    inner = {}
    for b in range(seqs):
        for g in range(groups):
            scores = 0.0
            for d in range(2):
                run = part(running[d], b, g)
                qd = part(q, b, g) * jnp.exp(run)
                ki = part(k, b, g) * jnp.exp(-run)
                decayed[b, g, d] = qd
                stack = jnp.concatenate([(ki * m).astype(bf16) for m in head_mask], axis=0)
                s = dot(qd.astype(bf16), stack, ((1,), (1,)))
                keep = t_row <= t_col if d else t_row >= t_col
                scores = scores + jnp.where(keep, s, 0.0)
            vb = part(v, b, g)
            v_stack = jnp.concatenate([vb * m for m in head_mask16], axis=0)
            inner[b, g] = dot(scores.astype(bf16), v_stack)

    for i in range(1, n_sp):
        src = lax.rem(sp + n_sp - i, n_sp)
        pltpu.make_async_remote_copy(
            src_ref=states.at[0],
            dst_ref=inbox.at[src],
            send_sem=sp_send_sem.at[i - 1],
            recv_sem=sp_recv_sem.at[src],
            device_id={"sp": src},
        ).wait_recv()

    block_row = lax.div(lax.broadcasted_iota(jnp.int32, (LANES, LANES), 0), HK)
    block_col = lax.div(lax.broadcasted_iota(jnp.int32, (LANES, LANES), 1), HK)
    block_ones = jnp.where(block_row == block_col, 1.0, 0.0).astype(bf16)
    gain = jnp.concatenate([ogain_v[...]] * heads, axis=1)
    attended = []
    for b in range(seqs):
        per_group = []
        for g in range(groups):
            box = [inbox[i, b * groups + g] for i in range(n_sp)]
            ends = [
                box[i][HK : HK + 1].astype(f32) + box[i][HK + 1 : HK + 2].astype(f32)
                for i in range(n_sp)
            ]
            between = [None] * n_sp
            run_f = jnp.zeros((1, LANES), f32)
            run_b = jnp.zeros((1, LANES), f32)
            pre_f = [None] * n_sp
            pre_b = [None] * n_sp
            for i in reversed(range(n_sp)):
                pre_f[i] = run_f
                run_f = run_f + jnp.where(sp > i, 1.0, 0.0) * ends[i]
            for i in range(n_sp):
                pre_b[i] = run_b
                run_b = run_b + jnp.where(sp < i, 1.0, 0.0) * ends[i]
            queries = []
            memory = []
            for i in range(n_sp):
                first = sp > i
                factor = jnp.exp(jnp.where(first, pre_f[i], pre_b[i]))
                base = jnp.where(first, decayed[b, g, 0], decayed[b, g, 1])
                queries.append((base * factor).astype(bf16))
                packed = box[i][:HK]
                memory += [packed * m for m in head_mask16]
            across = dot(jnp.concatenate(queries, axis=1), jnp.concatenate(memory, axis=0))
            out = inner[b, g] + across
            square = out * out
            high = square.astype(bf16)
            low = (square - high.astype(f32)).astype(bf16)
            mean = (dot(high, block_ones) + dot(low, block_ones)) * (1.0 / HK)
            per_group.append((out * lax.rsqrt(mean + EPS) * gain).astype(bf16))
        attended.append(jnp.concatenate(per_group, axis=1))
    arrive(4)
    mixed = dot(jnp.concatenate(attended, axis=0), wo[...]).astype(bf16)
    result[...] = mixed.reshape(seqs, toks, width)
    for copy in sends:
        copy.wait_send()


def solution(mesh):
    n_sp = mesh.shape["sp"]
    n_dp = mesh.shape["dp"]
    chips = n_dp // 2

    def per_device(
        tokens,
        norm_gain,
        w_query,
        w_key,
        w_value,
        w_rank_forward,
        w_rank_backward,
        up_forward,
        up_backward,
        bias_forward,
        bias_backward,
        out_gain,
        w_out,
    ):
        seqs, toks, width = tokens.shape
        depth, keys = w_query.shape
        rank = w_rank_forward.shape[1]
        groups = keys // LANES
        out_depth = w_out.shape[0]
        anywhere = pl.BlockSpec(memory_space=pl.ANY)
        return pl.pallas_call(
            functools.partial(kernel, n_sp, n_dp),
            out_shape=jax.ShapeDtypeStruct(tokens.shape, bf16),
            in_specs=[anywhere] * 13,
            out_specs=pl.BlockSpec(memory_space=pltpu.VMEM),
            scratch_shapes=[
                pltpu.VMEM((seqs, toks, width), bf16),
                pltpu.VMEM((1, width), f32),
                pltpu.VMEM((2, depth, rank), bf16),
                pltpu.VMEM((2, rank, keys), bf16),
                pltpu.VMEM((2, 1, keys), f32),
                pltpu.VMEM((1, HK), f32),
                pltpu.VMEM((n_dp, 2 * rank, depth), bf16),
                pltpu.VMEM((n_dp * depth, keys), bf16),
                pltpu.VMEM((n_dp * depth, keys), bf16),
                pltpu.VMEM((n_dp * depth, keys), bf16),
                pltpu.VMEM((n_dp * out_depth, width), bf16),
                pltpu.VMEM((2, seqs * groups, HK + 16, LANES), bf16),
                pltpu.VMEM((n_sp, seqs * groups, HK + 16, LANES), bf16),
                pltpu.SemaphoreType.DMA((13,)),
                pltpu.SemaphoreType.DMA((5, chips - 1)),
                pltpu.SemaphoreType.DMA((5, chips)),
                pltpu.SemaphoreType.DMA((5, n_dp)),
                pltpu.SemaphoreType.DMA((n_sp - 1,)),
                pltpu.SemaphoreType.DMA((n_sp,)),
            ],
            compiler_params=pltpu.CompilerParams(collective_id=0, has_side_effects=True),
        )(
            tokens,
            norm_gain.reshape(1, -1),
            w_query,
            w_key,
            w_value,
            w_rank_forward,
            w_rank_backward,
            up_forward,
            up_backward,
            bias_forward.reshape(1, -1),
            bias_backward.reshape(1, -1),
            out_gain.reshape(1, -1),
            w_out,
        )

    rows = P("dp", None)
    return jax.shard_map(
        per_device,
        mesh=mesh,
        in_specs=(P("dp", "sp", None), P(), rows, rows, rows, rows, rows, P(), P(), P(), P(), P(), rows),
        out_specs=P("dp", "sp", None),
        check_vma=False,
    )
```

time: 119 us -> 22.6 us (0.19)
  blocking collectives: 54.7 us -> 0 us
  starting transfers between devices: 24.5 us -> 0 us
  Pallas kernels: 0 us -> 18.6 us
  waiting for transfers between devices: 16.7 us -> 0 us
  local copies, waits for them, and re-layouts: 11.5 us -> 3.79 us
  matrix products: 7.7 us -> 0 us
  other arithmetic: 2.15 us -> 0 us
    all_gather x6 -> x0, blocking collectives: 54.7 us -> none  [over_all(): lax.all_gather(part, axis, axis=dim, tiled=True)]
    all_to_all x6 -> x0, starting transfers between devices: 24.5 us -> none  [the longest x1 5.09 us: per_device(): lax.all_to_all(for_sending(own_forward.reshape(seq_local, tok_local, -1))...]
    pallas_call x0 -> x1, Pallas kernels: none -> 18.6 us  [per_device(): pl.pallas_call(functools.partial(kernel, n_sp, n_dp), out_shape=jax.Shape...]
    all_to_all x6 -> x0, waiting for transfers between devices: 16.7 us -> none  [the longest x1 5.52 us: per_device(): lax.all_to_all(for_sending(own_forward.reshape(seq_local, tok_local, -1))...]
    dot_general x26 -> x0, matrix products: 7.7 us -> none  [the longest x8 1.86 us: advance(): emitted = jnp.einsum('hid,hdv->hiv', query_now, carried, precision=precise)]
    unnamed x40 -> x7, local copies, waits for them, and re-layouts: 7.47 us -> 3.79 us
  transfers between devices with their start and end apart: 6 -> 0, of which waited for: 4 -> 0; matrix products, arithmetic and copies ran while one was open for 9% -> 0% of each run, Pallas kernels for 0% -> 0%
where the time goes in v1:
time: 22.6 us; the launch traced here: 22.4 us
  Pallas kernels  18.6 us (82%)
  local copies, waits for them, and re-layouts  3.79 us (17%)
    pallas_call x1, Pallas kernels, per_device(): pl.pallas_call(functools.partial(kernel, n_sp, n_dp), out_shape=jax.Shape...  18.6 us
    unnamed x7, local copies, waits for them, and re-layouts  3.79 us

profile of v1, /device:TPU:0, one launch (start us, length us, event | category | flops | bytes accessed | tf_op | source)
XLA Modules:
  0.0 22.4 jit_solution(1658514335905508228)
XLA Ops:
  0.0 0.0 copy-start
  0.0 0.7 %copy-done = bf16[128,16]{0,1:T(8,128)(2,1)S(1)} copy-done((bf16[128,16]{0,1:T(8,128)(2,1)S(1)}, bf16[128,16]{0,1:T(8,128)(2,1)}, u32[]{:S(2)}) %copy-start) | copy-done | bytes 4120
  0.7 0.0 copy-start.1
  0.7 0.7 %copy.14.w_rank_f = bf16[128,16]{1,0:T(8,128)(2,1)} copy(bf16[128,16]{0,1:T(8,128)(2,1)S(1)} %copy-done) | data formatting | bytes 8192 | tf_op args[5]
  1.4 0.0 copy-done.1
  1.4 0.7 %copy.15.w_rank_b = bf16[128,16]{1,0:T(8,128)(2,1)} copy(bf16[128,16]{0,1:T(8,128)(2,1)S(1)} %copy-done.1) | data formatting | bytes 8192 | tf_op args[6]
  2.1 18.6 %shard_map.127 = bf16[2,64,1024]{2,1,0:T(8,128)(2,1)} custom-call(bf16[2,64,1024]{2,1,0:T(8,128)(2,1)} %tokens.1, f32[1,1024]{1,0:T(1,128)} %bitcast.4, bf16[128,128]{1,0:T(8,128)(2,1)} %w_query.1, bf16[128,128]{1,0:T(8,128)(2,1)} %w_key.1, bf16[128,128]{1,0:T(8,128)(2,1)} %w_value.1, bf16[128,16]{1,0:T(8,128)(2,1)} %copy.14.w_rank_f, ...), custom_call_target="tpu_custom_call" | custom-call | tf_op jit(solution)/shard_map/pallas_call | solution.py:326
  20.7 1.7 %copy.17 = bf16[2,64,1024]{2,1,0:T(8,128)(2,1)} copy(bf16[2,64,1024]{2,1,0:T(8,128)(2,1)} %shard_map.127) | data formatting | bytes 524288
Async XLA Ops:
  0.0 0.7 %copy-start = (bf16[128,16]{0,1:T(8,128)(2,1)S(1)}, bf16[128,16]{0,1:T(8,128)(2,1)}, u32[]{:S(2)}) copy-start(bf16[128,16]{0,1:T(8,128)(2,1)} %param.18) | copy-start | bytes 12292
  0.7 0.7 %copy-start.1 = (bf16[128,16]{0,1:T(8,128)(2,1)S(1)}, bf16[128,16]{0,1:T(8,128)(2,1)}, u32[]{:S(2)}) copy-start(bf16[128,16]{0,1:T(8,128)(2,1)} %param.19) | copy-start | bytes 12292

commit v2 on v1

--- a/solution.py
+++ b/solution.py
@@ -9,6 +9,7 @@
 
 HK = 32
 LANES = 128
+TAGS = 8
 EPS = 1e-06
 f32 = jnp.float32
 bf16 = jnp.bfloat16
@@ -18,9 +19,13 @@
     return lax.dot_general(a, b, (dims, ((), ())), preferred_element_type=f32)
 
 
+def in_two(a):
+    high = a.astype(bf16)
+    return high, (a - high.astype(f32)).astype(bf16)
+
+
 def split_dot(a, b):
-    high = b.astype(bf16)
-    low = (b - high.astype(f32)).astype(bf16)
+    high, low = in_two(b)
     return dot(a, high) + dot(a, low)
 
 
@@ -43,7 +48,6 @@
     result,
     tok_v,
     gain_v,
-    rank_v,
     up_v,
     bias_v,
     ogain_v,
@@ -72,7 +76,7 @@
     depth = w_query.shape[0]
     out_depth = w_out.shape[0]
     keys = w_query.shape[1]
-    rank = w_rank_f.shape[1]
+    rank = w_rank_f.shape[0]
     groups = keys // LANES
     heads = LANES // HK
 
@@ -93,8 +97,8 @@
 
     loads = []
     for src, dst in (
-        (w_rank_f, rank_v.at[0]),
-        (w_rank_b, rank_v.at[1]),
+        (w_rank_f, wr.at[dp, pl.ds(0, rank)]),
+        (w_rank_b, wr.at[dp, pl.ds(rank, rank)]),
         (w_key, slot(1, dp)),
         (w_value, slot(2, dp)),
         (w_query, slot(3, dp)),
@@ -113,7 +117,6 @@
     inbox[sp] = jnp.zeros(inbox.shape[1:], bf16)
     loads[0].wait()
     loads[1].wait()
-    wr[dp] = jnp.concatenate([rank_v[0].astype(f32).T, rank_v[1].astype(f32).T], axis=0).astype(bf16)
     pl.semaphore_wait(barrier, len(far) + 1 + len(peers))
 
     def remote(which, src, sem, target):
@@ -166,6 +169,7 @@
     upper = jnp.where(same & (row <= col), 1.0, 0.0).astype(bf16)
 
     relay(0)
+    relay(1)
     arrive(0)
     w_ranks = jnp.concatenate([wr[s] for s in range(n_dp)], axis=1)
     ranks = dot(normed, w_ranks, ((1,), (1,))).astype(bf16)
@@ -175,29 +179,35 @@
         logits = dot(ranks[:, d * rank : (d + 1) * rank], up_v[d]) + bias_v[d]
         rates = (jnp.minimum(logits, 0.0) - jnp.log1p(jnp.exp(-jnp.abs(logits)))) * scale
         running.append(split_dot(upper if d else lower, rates))
-    relay(1)
+    relay(2)
     arrive(1)
     k = dot(normed, wk[...]).astype(bf16).astype(f32)
-    relay(2)
-    arrive(2)
-    v = dot(normed, wv[...]).astype(bf16)
-
-    lane = lax.broadcasted_iota(jnp.int32, (1, LANES), 1)
-    head_mask = [jnp.where(lax.div(lane, HK) == h, 1.0, 0.0) for h in range(heads)]
-    head_mask16 = [m.astype(bf16) for m in head_mask]
-    tag_row = lax.broadcasted_iota(jnp.int32, (16, LANES), 0)
 
     def part(a, b, g):
         return a[b * toks : (b + 1) * toks, g * LANES : (g + 1) * LANES]
 
-    closing = {}
+    remain = {}
+    ends = {}
     for b in range(seqs):
         for g in range(groups):
             for d in range(2):
                 run = part(running[d], b, g)
                 end = run[:1] if d else run[toks - 1 :]
-                remain = (part(k, b, g) * jnp.exp(end - run)).astype(bf16)
-                summary = dot(remain, part(v, b, g), ((0,), (0,)))
+                ends[b, g, d] = end
+                remain[b, g, d] = (part(k, b, g) * jnp.exp(end - run)).astype(bf16)
+    arrive(2)
+    v = dot(normed, wv[...]).astype(bf16)
+
+    lane = lax.broadcasted_iota(jnp.int32, (1, LANES), 1)
+    head_mask = [jnp.where(lax.div(lane, HK) == h, 1.0, 0.0) for h in range(heads)]
+    head_mask16 = [m.astype(bf16) for m in head_mask]
+    tag_row = lax.broadcasted_iota(jnp.int32, (TAGS, LANES), 0)
+
+    for b in range(seqs):
+        for g in range(groups):
+            for d in range(2):
+                end = ends[b, g, d]
+                summary = dot(remain[b, g, d], part(v, b, g), ((0,), (0,)))
                 packed = sum(summary[h * HK : (h + 1) * HK] * head_mask[h] for h in range(heads))
                 high = end.astype(bf16).astype(f32)
                 tags = jnp.where(tag_row == 0, high, jnp.where(tag_row == 1, end - high, 0.0))
@@ -231,13 +241,21 @@
                 qd = part(q, b, g) * jnp.exp(run)
                 ki = part(k, b, g) * jnp.exp(-run)
                 decayed[b, g, d] = qd
-                stack = jnp.concatenate([(ki * m).astype(bf16) for m in head_mask], axis=0)
-                s = dot(qd.astype(bf16), stack, ((1,), (1,)))
+                q_high, q_low = in_two(qd)
+                k_high, k_low = in_two(ki)
+                high = jnp.concatenate([k_high * m for m in head_mask16], axis=0)
+                low = jnp.concatenate([k_low * m for m in head_mask16], axis=0)
+                s = dot(
+                    jnp.concatenate([q_high, q_low, q_high], axis=1),
+                    jnp.concatenate([high, high, low], axis=1),
+                    ((1,), (1,)),
+                )
                 keep = t_row <= t_col if d else t_row >= t_col
                 scores = scores + jnp.where(keep, s, 0.0)
             vb = part(v, b, g)
             v_stack = jnp.concatenate([vb * m for m in head_mask16], axis=0)
-            inner[b, g] = dot(scores.astype(bf16), v_stack)
+            s_high, s_low = in_two(scores)
+            inner[b, g] = dot(s_high, v_stack) + dot(s_low, v_stack)
 
     for i in range(1, n_sp):
         src = lax.rem(sp + n_sp - i, n_sp)
@@ -258,21 +276,20 @@
         per_group = []
         for g in range(groups):
             box = [inbox[i, b * groups + g] for i in range(n_sp)]
-            ends = [
+            tails = [
                 box[i][HK : HK + 1].astype(f32) + box[i][HK + 1 : HK + 2].astype(f32)
                 for i in range(n_sp)
             ]
-            between = [None] * n_sp
             run_f = jnp.zeros((1, LANES), f32)
             run_b = jnp.zeros((1, LANES), f32)
             pre_f = [None] * n_sp
             pre_b = [None] * n_sp
             for i in reversed(range(n_sp)):
                 pre_f[i] = run_f
-                run_f = run_f + jnp.where(sp > i, 1.0, 0.0) * ends[i]
+                run_f = run_f + jnp.where(sp > i, 1.0, 0.0) * tails[i]
             for i in range(n_sp):
                 pre_b[i] = run_b
-                run_b = run_b + jnp.where(sp < i, 1.0, 0.0) * ends[i]
+                run_b = run_b + jnp.where(sp < i, 1.0, 0.0) * tails[i]
             queries = []
             memory = []
             for i in range(n_sp):
@@ -331,7 +348,6 @@
             scratch_shapes=[
                 pltpu.VMEM((seqs, toks, width), bf16),
                 pltpu.VMEM((1, width), f32),
-                pltpu.VMEM((2, depth, rank), bf16),
                 pltpu.VMEM((2, rank, keys), bf16),
                 pltpu.VMEM((2, 1, keys), f32),
                 pltpu.VMEM((1, HK), f32),
@@ -340,8 +356,8 @@
                 pltpu.VMEM((n_dp * depth, keys), bf16),
                 pltpu.VMEM((n_dp * depth, keys), bf16),
                 pltpu.VMEM((n_dp * out_depth, width), bf16),
-                pltpu.VMEM((2, seqs * groups, HK + 16, LANES), bf16),
-                pltpu.VMEM((n_sp, seqs * groups, HK + 16, LANES), bf16),
+                pltpu.VMEM((2, seqs * groups, HK + TAGS, LANES), bf16),
+                pltpu.VMEM((n_sp, seqs * groups, HK + TAGS, LANES), bf16),
                 pltpu.SemaphoreType.DMA((13,)),
                 pltpu.SemaphoreType.DMA((5, chips - 1)),
                 pltpu.SemaphoreType.DMA((5, chips)),
@@ -356,8 +372,8 @@
             w_query,
             w_key,
             w_value,
-            w_rank_forward,
-            w_rank_backward,
+            w_rank_forward.T,
+            w_rank_backward.T,
             up_forward,
             up_backward,
             bias_forward.reshape(1, -1),

time: 22.6 us -> 19.6 us (0.87)
  local copies, waits for them, and re-layouts: 3.79 us -> 1.67 us
  Pallas kernels: 18.6 us -> 17.8 us
    unnamed x7 -> x1, local copies, waits for them, and re-layouts: 3.79 us -> 1.67 us
    pallas_call x1, Pallas kernels: 18.6 us -> 17.8 us  [per_device(): pl.pallas_call(functools.partial(kernel, n_sp, n_dp), out_shape=jax.Shape...]
where the time goes in v2:
time: 19.6 us; the launch traced here: 19.4 us
  Pallas kernels  17.8 us (91%)
  local copies, waits for them, and re-layouts  1.67 us (9%)
    pallas_call x1, Pallas kernels, per_device(): pl.pallas_call(functools.partial(kernel, n_sp, n_dp), out_shape=jax.Shape...  17.8 us
    unnamed x1, local copies, waits for them, and re-layouts  1.67 us

profile of v2, /device:TPU:0, one launch (start us, length us, event | category | flops | bytes accessed | tf_op | source)
XLA Modules:
  0.0 19.4 jit_solution(15506069817580600948)
XLA Ops:
  0.0 17.8 %shard_map.127 = bf16[2,64,1024]{2,1,0:T(8,128)(2,1)} custom-call(bf16[2,64,1024]{2,1,0:T(8,128)(2,1)} %tokens.1, f32[1,1024]{1,0:T(1,128)} %bitcast.6, bf16[128,128]{1,0:T(8,128)(2,1)} %w_query.1, bf16[128,128]{1,0:T(8,128)(2,1)} %w_key.1, bf16[128,128]{1,0:T(8,128)(2,1)} %w_value.1, bf16[16,128]{1,0:T(8,128)(2,1)} %bitcast.7, bf16[16,128]{1,0:T(8,128)(2,1)} %bitcast.8, ...), custom_call_target="tpu_custom_call" | custom-call | tf_op jit(solution)/shard_map/pallas_call | solution.py:343
  17.8 1.7 %copy.15 = bf16[2,64,1024]{2,1,0:T(8,128)(2,1)} copy(bf16[2,64,1024]{2,1,0:T(8,128)(2,1)} %shard_map.127) | data formatting | bytes 524288
